TPU v7x, 32 devices: a whole 2x2x4 slice. The times are simulated.
32 devices in a mesh: ep: 32 (over z, y, x, core).
Axes of the slice: x: 2, y: 2, z: 4, core: 2. Of those that a mesh axis runs over, the one named last changes fastest.
Arguments:
- tokens: bfloat16 [512, 1024], P('ep'), may hold values from -6 to 6
- lengths: int32 [512], P('ep'), may hold values from 1 to 8191
- cache_keys: bfloat16 [512, 128, 512], P('ep'), may hold values from -6 to 6
- cache_values: bfloat16 [512, 128, 1024], P('ep'), may hold values from -6 to 6
- retention_state: float32 [512, 4, 128, 256], P('ep'), may hold values from -24 to 24
- mix_gain: float32 [1024], replicated, may hold values from 0.1 to 1.9
- query_weight: bfloat16 [1024, 512], replicated, may hold values from -0.1875 to 0.1875
- key_weight: bfloat16 [1024, 512], replicated, may hold values from -0.1875 to 0.1875
- value_weight: bfloat16 [1024, 1024], replicated, may hold values from -0.1875 to 0.1875
- out_weight: bfloat16 [1024, 1024], replicated, may hold values from -0.1875 to 0.1875
- ffn_gain: float32 [1024], replicated, may hold values from 0.1 to 1.9
- routes: int32 [512, 6], P('ep'), may hold values from 0 to 31, all different within a row; in each aligned block of 16 rows (0 to 15, 16 to 31, ...) at most 8 rows name the same one
- route_scores: float32 [512, 6], P('ep'), may hold values from 0.05 to 1
- expert_gate: bfloat16 [32, 1024, 256], P('ep'), may hold values from -0.1875 to 0.1875
- expert_up: bfloat16 [32, 1024, 256], P('ep'), may hold values from -0.1875 to 0.1875
- expert_down: bfloat16 [32, 256, 1024], P('ep'), may hold values from -0.375 to 0.375
- shared_gate: bfloat16 [1024, 256], replicated, may hold values from -0.1875 to 0.1875
- shared_up: bfloat16 [1024, 256], replicated, may hold values from -0.1875 to 0.1875
- shared_down: bfloat16 [256, 1024], replicated, may hold values from -0.375 to 0.375
- dense_gate: bfloat16 [4096, 1024], P('ep'), may hold values from -0.1875 to 0.1875
- dense_up: bfloat16 [4096, 1024], P('ep'), may hold values from -0.1875 to 0.1875
- dense_down: bfloat16 [4096, 1024], P('ep'), may hold values from -0.09375 to 0.09375
- dense_mix: float32 [1024], replicated, may hold values from -3 to 3
Outputs:
- layer_out: bfloat16 [512, 1024], P('ep')
- new_keys: bfloat16 [512, 512], P('ep')
- new_values: bfloat16 [512, 1024], P('ep')
Inputs may be any that keep to these rules, and one draw needn't show every extreme that they name: `routes`: each row names 6 different experts; among the rows of one device no expert is named more than 8 times.
All inputs are finite; a program needn't handle non-finite values.
Results may differ from a plain program's by a relative error of at most 0.012.
Values may be sent and summed in bfloat16 or wider, within the bound.
A program may use at most 128 MiB of HBM per device.

v0:
```python
import jax
import jax.numpy as jnp
from jax import lax
from jax.sharding import PartitionSpec as P

eps = 1e-06
route_scale = 2.5
rope_base = 10000.0


def normed(values):
    return values * lax.rsqrt(jnp.mean(values * values, axis=-1, keepdims=True) + eps)


def log_decay(head_count):
    return jnp.log1p(-jnp.exp2(-5.0 - jnp.arange(head_count, dtype=jnp.float32)))


def rotate(values, positions):
    half_size = values.shape[-1] // 2
    inverse = rope_base ** (-jnp.arange(half_size, dtype=jnp.float32) / half_size)
    angles = positions.astype(jnp.float32)[:, None, None] * inverse[None, None, :]
    cosine = jnp.cos(angles)
    sine_part = jnp.sin(angles)
    first_half = values[..., :half_size]
    second = values[..., half_size:]
    return jnp.concatenate(
        [first_half * cosine - second * sine_part, first_half * sine_part + second * cosine],
        axis=-1,
    )


def swiglu(inputs, w_gate, w_up, w_down):
    gate_part = jnp.dot(inputs, w_gate, preferred_element_type=jnp.float32)
    up_part = jnp.dot(inputs, w_up, preferred_element_type=jnp.float32)
    hidden = (jax.nn.silu(gate_part) * up_part).astype(jnp.bfloat16)
    return jnp.dot(hidden, w_down, preferred_element_type=jnp.float32)


def dense_part(inputs, gate_rows, up_rows, down_rows):
    contract = (((1,), (1,)), ((), ()))
    gate_part = lax.dot_general(inputs, gate_rows, contract, preferred_element_type=jnp.float32)
    up_part = lax.dot_general(inputs, up_rows, contract, preferred_element_type=jnp.float32)
    hidden = (jax.nn.silu(gate_part) * up_part).astype(jnp.bfloat16)
    return jnp.dot(hidden, down_rows, preferred_element_type=jnp.float32)


def retain(
    tokens, lengths, mix_gain, w_query, w_key, w_value, w_out, cache_keys, cache_values, carry_state
):
    seq_count, head_count, key_size, value_size = carry_state.shape
    block_size = cache_keys.shape[1]
    widened = tokens.astype(jnp.float32)
    normal_in = (normed(widened) * mix_gain).astype(jnp.bfloat16)
    raw_query = jnp.dot(normal_in, w_query, preferred_element_type=jnp.float32).reshape(
        seq_count, head_count, key_size
    )
    raw_key = jnp.dot(normal_in, w_key, preferred_element_type=jnp.float32).reshape(
        seq_count, head_count, key_size
    )
    raw_value = jnp.dot(normal_in, w_value, preferred_element_type=jnp.float32).reshape(
        seq_count, head_count, value_size
    )
    queries = (rotate(raw_query, lengths) * key_size ** (-0.5)).astype(jnp.bfloat16)
    new_keys = rotate(raw_key, lengths).astype(jnp.bfloat16)
    new_values = raw_value.astype(jnp.bfloat16)
    filled = lengths % block_size
    decay_rate = log_decay(head_count)
    places = jnp.arange(block_size, dtype=jnp.int32)
    stored_keys = cache_keys.reshape(seq_count, block_size, head_count, key_size)
    stored_values = cache_values.reshape(seq_count, block_size, head_count, value_size)
    scores = jnp.einsum("shd,sjhd->shj", queries, stored_keys, preferred_element_type=jnp.float32)
    distance = jnp.maximum(filled[:, None] - places[None, :], 0).astype(jnp.float32)
    live_mask = places[None, :] < filled[:, None]
    weighted = jnp.where(
        live_mask[:, None, :],
        scores * jnp.exp(distance[:, None, :] * decay_rate[None, :, None]),
        0.0,
    ).astype(jnp.bfloat16)
    own_weight = jnp.sum(
        queries.astype(jnp.float32) * new_keys.astype(jnp.float32), axis=-1
    ).astype(jnp.bfloat16)
    inside = jnp.einsum(
        "shj,sjhe->she", weighted, stored_values, preferred_element_type=jnp.float32
    )
    inside = inside + own_weight.astype(jnp.float32)[:, :, None] * new_values.astype(jnp.float32)
    carried = jnp.einsum(
        "shd,shde->she", queries.astype(jnp.float32), carry_state, precision=lax.Precision.HIGHEST
    )
    carried = (
        carried
        * jnp.exp((filled.astype(jnp.float32)[:, None] + 1.0) * decay_rate[None, :])[:, :, None]
    )
    headed = (
        normed(inside + carried).astype(jnp.bfloat16).reshape(seq_count, head_count * value_size)
    )
    mixer_out = jnp.dot(headed, w_out, preferred_element_type=jnp.float32)
    residual = widened + normed(mixer_out)
    return (
        residual,
        new_keys.reshape(seq_count, head_count * key_size),
        new_values.reshape(seq_count, head_count * value_size),
    )


def capacity(seq_count, top_count, expert_count):
    return max(2, seq_count * top_count * 8 // (3 * expert_count))


def gather_tokens(normal_ffn):
    return lax.all_gather(normal_ffn, "ep", axis=0, tiled=True)


def branch_sums(term_rows, seq_count):
    return lax.psum_scatter(
        term_rows(jnp.int32(0), seq_count * lax.axis_size("ep")),
        "ep",
        scatter_dimension=0,
        tiled=True,
    )


def exchanged_experts(normal_ffn, routes, route_weight, expert_gate, expert_up, expert_down):
    seq_count, top_count = routes.shape
    model_width = normal_ffn.shape[1]
    expert_count = lax.axis_size("ep") * expert_gate.shape[0]
    slot_count = capacity(seq_count, top_count, expert_count)
    flat_routes = routes.reshape(-1)
    onehot = (flat_routes[:, None] == jnp.arange(expert_count, dtype=jnp.int32)[None, :]).astype(
        jnp.int32
    )
    slot_ids = jnp.sum((jnp.cumsum(onehot, axis=0) - 1) * onehot, axis=1)
    target = flat_routes * slot_count + slot_ids
    placed = (
        target[None, :] == jnp.arange(expert_count * slot_count, dtype=jnp.int32)[:, None]
    ).astype(jnp.float32)
    chosen = jnp.sum(placed.reshape(expert_count * slot_count, seq_count, top_count), axis=2)
    outgoing = jnp.dot(
        chosen.astype(jnp.bfloat16), normal_ffn, preferred_element_type=jnp.float32
    ).astype(jnp.bfloat16)
    outgoing = outgoing.reshape(expert_count, slot_count, model_width)
    arrived = lax.all_to_all(outgoing, "ep", split_axis=0, concat_axis=0, tiled=True)
    outputs = swiglu(
        arrived.reshape(-1, model_width), expert_gate[0], expert_up[0], expert_down[0]
    ).astype(jnp.bfloat16)
    returned = lax.all_to_all(
        outputs.reshape(arrived.shape), "ep", split_axis=0, concat_axis=0, tiled=True
    )
    weights_by_slot = placed * route_weight.reshape(-1)[None, :]
    combine = jnp.sum(
        weights_by_slot.reshape(expert_count * slot_count, seq_count, top_count), axis=2
    )
    return lax.dot_general(
        combine,
        returned.reshape(-1, model_width).astype(jnp.float32),
        (((0,), (0,)), ((), ())),
        precision=lax.Precision.HIGHEST,
    )


def per_device(
    tokens,
    lengths,
    cache_keys,
    cache_values,
    retention_state,
    mix_gain,
    query_weight,
    key_weight,
    value_weight,
    out_weight,
    ffn_gain,
    routes,
    route_scores,
    expert_gate,
    expert_up,
    expert_down,
    shared_gate,
    shared_up,
    shared_down,
    dense_gate,
    dense_up,
    dense_down,
    dense_mix,
):
    residual, new_keys, new_values = retain(
        tokens,
        lengths,
        mix_gain,
        query_weight,
        key_weight,
        value_weight,
        out_weight,
        cache_keys,
        cache_values,
        retention_state,
    )
    normal_ffn = (normed(residual) * ffn_gain).astype(jnp.bfloat16)
    seq_count, top_count = routes.shape
    shared_out = swiglu(normal_ffn, shared_gate, shared_up, shared_down)
    gated = jax.nn.sigmoid(dense_mix)
    route_weight = route_scores / jnp.sum(route_scores, axis=-1, keepdims=True) * route_scale
    gathered = gather_tokens(normal_ffn)

    def dense_rows(row_start, row_count):
        return gated * dense_part(gathered, dense_gate, dense_up, dense_down)

    combined = (
        shared_out
        + branch_sums(dense_rows, seq_count)
        + exchanged_experts(normal_ffn, routes, route_weight, expert_gate, expert_up, expert_down)
    )
    layer_out = (residual + normed(combined)).astype(jnp.bfloat16)
    return (layer_out, new_keys, new_values)


def solution(mesh):
    in_specs = (
        P("ep", None),
        P("ep"),
        P("ep", None, None),
        P("ep", None, None),
        P("ep", None, None, None),
        P(),
        P(),
        P(),
        P(),
        P(),
        P(),
        P("ep", None),
        P("ep", None),
        P("ep", None, None),
        P("ep", None, None),
        P("ep", None, None),
        P(),
        P(),
        P(),
        P("ep", None),
        P("ep", None),
        P("ep", None),
        P(),
    )
    out_specs = (P("ep", None), P("ep", None), P("ep", None))
    return jax.shard_map(
        per_device, mesh=mesh, in_specs=in_specs, out_specs=out_specs, check_vma=False
    )
```

profile of v0, /device:TPU:0, one launch (start us, length us, event | category | flops | bytes accessed | tf_op | source)
XLA Modules:
  0.0 239.3 jit_solution(18179458342406826511)
XLA Ops:
  7.2 0.0 copy-start
  7.2 0.0 copy-start.4
  7.2 0.0 copy-start.7
  7.2 0.0 all-gather.2.cloned.1.call-start
  7.3 0.8 convert_add_fusion.1
  8.1 0.7 convert_element_type.102
  8.7 0.1 maximum_convert_fusion.1
  8.8 0.1 iota_compare_fusion.2
  8.9 0.9 fusion.29
  9.8 1.6 fusion.53
  11.4 1.5 fusion.55
  12.9 0.1 multiply_cosine_fusion
  13.0 0.1 multiply_subtract_fusion
  13.1 0.1 multiply_subtract_fusion.1
  13.2 0.0 copy-done.4
  13.2 0.0 copy-done.7
  13.3 2.0 convolution_convert_fusion.2
  15.3 0.2 multiply_reduce_fusion.4
  15.5 3.9 %copy.44 = bf16[16,128,512]{1,2,0:T(8,128)(2,1)} copy(bf16[16,128,512]{2,1,0:T(8,128)(2,1)} %param.25) | data formatting | bytes 4194304 | tf_op jit(solution)/shard_map/reshape | solution.py:70
  19.5 0.0 copy-done.6
  19.5 6.3 %fusion.36 = f32[16,4,1,256]{3,2,1,0:T(1,128)S(1)} fusion(f32[16,4,128,256]{3,2,1,0:T(8,128)} %param.27, bf16[16,4,128,1]{2,1,0,3:T(4,128)(2,1)S(1)} %bitcast.73), kind=kOutput, calls=%fused_computation.68 | convolution fusion | flops 25165824 | bytes 8470528 | tf_op jit(solution)/shard_map/shd,shde->she/dot_general | solution.py:87
  25.7 0.0 copy-done.1
  25.7 0.6 fusion.38
  26.4 0.1 multiply_exponential_fusion
  26.4 0.1 fusion.40
  26.6 0.0 copy-done.3
  26.6 0.7 fusion
  27.2 0.2 multiply_reduce_fusion.3
  27.4 0.1 multiply_convert_fusion.1
  27.5 0.0 copy-done
  27.5 0.5 multiply_reduce_fusion.2
  28.1 0.2 multiply_reduce_fusion.1
  28.3 0.0 copy-done.10
  28.3 0.7 multiply_convert_fusion
  29.0 0.0 all-gather.2.cloned.1.call-update
  29.0 0.0 reduce-scatter.2.cloned.1.call-start
  29.0 0.0 copy-done.11
  29.1 56.4 %all-gather.2.cloned.1.call-done = bf16[512,1024]{1,0:T(8,128)(2,1)} async-done(((bf16[16,1024]{1,0:T(8,128)(2,1)}), bf16[512,1024]{1,0:T(8,128)(2,1)}) %all-gather.2.cloned.1.call-update) | async-done | bytes 1048592 | tf_op jit(solution)/shard_map/all_gather | solution.py:111
  85.5 1.8 fusion.60
  87.3 0.0 copy-done.2
  87.3 0.0 copy-start.8
  87.3 3.6 %convolution_multiply_fusion = f32[512,1024]{1,0:T(8,128)} fusion(bf16[128,1024]{1,0:T(8,128)(2,1)} %param.44, bf16[512,1024]{1,0:T(8,128)(2,1)S(1)} %copy-done.2, bf16[128,1024]{1,0:T(8,128)(2,1)} %param.43, f32[1024]{0:T(1024)S(1)} %add_divide_fusion, f32[512,128]{1,0:T(8,128)S(1)} %fusion.60), kind=kOutput, calls=%fused_computation.3 | convolution fusion | flops 269352960 | bytes 3936256 | tf_op jit(solution)/shard_map/dot_general | solution.py:45
  90.9 0.0 reduce-scatter.2.cloned.1.call-update
  90.9 0.0 copy-done.8
  90.9 0.1 copy.35
  91.0 0.1 eq.32
  91.1 0.1 fusion.33
  91.2 0.1 reduce_window_sum.11
  91.3 0.2 select_reduce_fusion.1
  91.5 0.1 reduce_sum.98
  91.6 0.1 copy.36
  91.8 0.1 convert_reduce_fusion
  91.9 0.3 fusion.3
  92.2 20.1 %all_to_all.10 = bf16[32,8,1024]{2,1,0:T(8,128)(2,1)S(1)} all-to-all(bf16[32,8,1024]{2,1,0:T(8,128)(2,1)S(1)} %fusion.3), channel_id=1, replica_groups=mesh['ep'=32] {'ep'}, dimensions={0} | all-to-all | bytes 1048576 | tf_op jit(solution)/shard_map/all_to_all | solution.py:142
  112.2 1.3 fusion.12
  113.6 2.8 %fusion.4 = bf16[32,8,1024]{2,1,0:T(8,128)(2,1)} fusion(bf16[1,256,1024]{2,1,0:T(8,128)(2,1)} %param.38, bf16[1,1024,256]{2,1,0:T(8,128)(2,1)} %param.37, bf16[32,8,1024]{2,1,0:T(8,128)(2,1)S(1)} %all_to_all.10, f32[256,256]{1,0:T(8,128)S(1)} %fusion.12), kind=kOutput, calls=%fused_computation.7 | convolution fusion | flops 269090816 | bytes 2359296 | tf_op jit(solution)/shard_map/dot_general | solution.py:37
  116.3 2.9 %all-to-all-start.1 = ((bf16[32,8,1024]{2,1,0:T(8,128)(2,1)}), bf16[32,8,1024]{2,1,0:T(8,128)(2,1)S(1)}, u32[]{:S(2)}, u32[]{:S(2)}) async-start(bf16[32,8,1024]{2,1,0:T(8,128)(2,1)} %fusion.4), calls=%async_computation.2 | async-start | bytes 1048576 | tf_op jit(solution)/shard_map/all_to_all | solution.py:146
  119.2 0.6 copy.63
  119.8 1.2 fusion.59
  121.1 108.6 %reduce-scatter.2.cloned.1.call-done = f32[16,1024]{1,0:T(8,128)} async-done(((f32[512,1024]{1,0:T(8,128)}), f32[16,1024]{1,0:T(8,128)}) %reduce-scatter.2.cloned.1.call-update) | async-done | bytes 65552 | tf_op jit(solution)/shard_map/reduce_scatter | solution.py:115
  229.7 1.7 convolution_add_fusion.1
  231.3 0.0 all-to-all-done.1
  231.3 0.4 multiply_reduce_fusion
  231.8 0.7 add_convert_fusion
  (26 shorter events, 0.2 us)
Async XLA Ops:
  7.2 20.4 %copy-start = (bf16[1024,1024]{1,0:T(8,128)(2,1)S(1)}, bf16[1024,1024]{1,0:T(8,128)(2,1)}, u32[]{:S(2)}) copy-start(bf16[1024,1024]{1,0:T(8,128)(2,1)} %param.32) | copy-start | bytes 6291460
  7.2 6.1 %copy-start.4 = (bf16[16,1024]{1,0:T(8,128)(2,1)S(1)}, bf16[16,1024]{1,0:T(8,128)(2,1)}, u32[]{:S(2)}) copy-start(bf16[16,1024]{1,0:T(8,128)(2,1)} %param.23) | copy-start | bytes 98308
  7.2 6.1 %copy-start.7 = (f32[1024]{0:T(1024)S(1)}, f32[1024]{0:T(1024)}, u32[]{:S(2)}) copy-start(f32[1024]{0:T(1024)} %param.28) | copy-start | bytes 12292
  7.2 78.3 %all-gather.2.cloned.1.call-start = ((), (), s32[]{:S(2)}) async-start(), calls=%async_computation.3 | async-start | bytes 1081344 | tf_op jit(solution)/shard_map/all_gather | solution.py:111
  15.3 4.2 %copy-start.6 = (bf16[16,1024]{1,0:T(8,128)(2,1)}, bf16[16,1024]{1,0:T(8,128)(2,1)S(1)}, u32[]{:S(2)}) copy-start(bf16[16,1024]{1,0:T(8,128)(2,1)S(1)} %convolution_convert_fusion.2) | copy-start | bytes 98308
  19.5 6.3 %copy-start.1 = (bf16[16,128,512]{1,2,0:T(8,128)(2,1)S(1)}, bf16[16,128,512]{1,2,0:T(8,128)(2,1)}, u32[]{:S(2)}) copy-start(bf16[16,128,512]{1,2,0:T(8,128)(2,1)} %copy.44) | copy-start | bytes 6291460
  19.5 7.1 %copy-start.3 = (bf16[16,128,1024]{2,1,0:T(8,128)(2,1)S(1)}, bf16[16,128,1024]{2,1,0:T(8,128)(2,1)}, u32[]{:S(2)}) copy-start(bf16[16,128,1024]{2,1,0:T(8,128)(2,1)} %param.26) | copy-start | bytes 12582916
  27.2 1.1 copy-start.10
  27.2 1.8 copy-start.11
  29.0 200.7 %reduce-scatter.2.cloned.1.call-start = ((), (), s32[]{:S(2)}) async-start(), calls=%async_computation.4 | async-start | bytes 2162688 | tf_op jit(solution)/shard_map/reduce_scatter | solution.py:115
  85.5 1.8 copy-start.2
  87.3 3.6 %copy-start.8 = (s32[16,6]{0,1:T(8,128)S(1)}, s32[16,6]{0,1:T(8,128)}, u32[]{:S(2)}) copy-start(s32[16,6]{0,1:T(8,128)} %param.34) | copy-start | bytes 1156
  90.9 0.8 copy-start.9
  90.9 0.9 copy-start.5
  116.3 115.0 %all-to-all-start.1 = ((bf16[32,8,1024]{2,1,0:T(8,128)(2,1)}), bf16[32,8,1024]{2,1,0:T(8,128)(2,1)S(1)}, u32[]{:S(2)}, u32[]{:S(2)}) async-start(bf16[32,8,1024]{2,1,0:T(8,128)(2,1)} %fusion.4), calls=%async_computation.2 | async-start | bytes 1048576 | tf_op jit(solution)/shard_map/all_to_all | solution.py:146
Sparse Core Ops, SparseCore 0:
  29.1 56.3 all-gather.1
  91.1 138.5 reduce-scatter.1
where the time goes:
time: 240 us; the launch traced here: 239 us
  waiting for transfers between devices  165 us (69%)
  matrix products  26.3 us (11%)
  blocking collectives  20.1 us (8%)
  between operations  14.3 us (6%)
  other arithmetic  5.61 us (2%)
  local copies, waits for them, and re-layouts  5.02 us (2%)
  starting transfers between devices  2.96 us (1%)
    reduce_scatter x1, waiting for transfers between devices, branch_sums(): lax.psum_scatter(term_rows(jnp.int32(0), seq_count * lax.axis_size('ep'))...  109 us
    all_gather x1, waiting for transfers between devices, gather_tokens(): return lax.all_gather(normal_ffn, 'ep', axis=0, tiled=True)  56.4 us
    all_to_all x1, blocking collectives, exchanged_experts(): lax.all_to_all(outgoing, 'ep', split_axis=0, concat_axis=0, tiled=True)  20.1 us
    dot_general x1, matrix products, retain(): jnp.einsum('shd,shde->she', queries.astype(jnp.float32), carry_state, pre...  6.26 us
  transfers between devices with their start and end apart: 3, of which 2 were waited for; matrix products, arithmetic and copies ran while one was open for 4% of the time, Pallas kernels for 0%

commit v1 on v0

--- a/solution.py
+++ b/solution.py
@@ -1,6 +1,11 @@
+import functools
+import math
+
 import jax
 import jax.numpy as jnp
 from jax import lax
+from jax.experimental import pallas as pl
+from jax.experimental.pallas import tpu as pltpu
 from jax.sharding import PartitionSpec as P
 
 eps = 1e-06
@@ -28,21 +33,6 @@
         [first_half * cosine - second * sine_part, first_half * sine_part + second * cosine],
         axis=-1,
     )
-
-
-def swiglu(inputs, w_gate, w_up, w_down):
-    gate_part = jnp.dot(inputs, w_gate, preferred_element_type=jnp.float32)
-    up_part = jnp.dot(inputs, w_up, preferred_element_type=jnp.float32)
-    hidden = (jax.nn.silu(gate_part) * up_part).astype(jnp.bfloat16)
-    return jnp.dot(hidden, w_down, preferred_element_type=jnp.float32)
-
-
-def dense_part(inputs, gate_rows, up_rows, down_rows):
-    contract = (((1,), (1,)), ((), ()))
-    gate_part = lax.dot_general(inputs, gate_rows, contract, preferred_element_type=jnp.float32)
-    up_part = lax.dot_general(inputs, up_rows, contract, preferred_element_type=jnp.float32)
-    hidden = (jax.nn.silu(gate_part) * up_part).astype(jnp.bfloat16)
-    return jnp.dot(hidden, down_rows, preferred_element_type=jnp.float32)
 
 
 def retain(
@@ -103,59 +93,374 @@
     )
 
 
-def capacity(seq_count, top_count, expert_count):
-    return max(2, seq_count * top_count * 8 // (3 * expert_count))
-
-
-def gather_tokens(normal_ffn):
-    return lax.all_gather(normal_ffn, "ep", axis=0, tiled=True)
-
-
-def branch_sums(term_rows, seq_count):
-    return lax.psum_scatter(
-        term_rows(jnp.int32(0), seq_count * lax.axis_size("ep")),
-        "ep",
-        scatter_dimension=0,
-        tiled=True,
-    )
-
-
-def exchanged_experts(normal_ffn, routes, route_weight, expert_gate, expert_up, expert_down):
-    seq_count, top_count = routes.shape
-    model_width = normal_ffn.shape[1]
-    expert_count = lax.axis_size("ep") * expert_gate.shape[0]
-    slot_count = capacity(seq_count, top_count, expert_count)
-    flat_routes = routes.reshape(-1)
-    onehot = (flat_routes[:, None] == jnp.arange(expert_count, dtype=jnp.int32)[None, :]).astype(
-        jnp.int32
-    )
-    slot_ids = jnp.sum((jnp.cumsum(onehot, axis=0) - 1) * onehot, axis=1)
-    target = flat_routes * slot_count + slot_ids
-    placed = (
-        target[None, :] == jnp.arange(expert_count * slot_count, dtype=jnp.int32)[:, None]
-    ).astype(jnp.float32)
-    chosen = jnp.sum(placed.reshape(expert_count * slot_count, seq_count, top_count), axis=2)
-    outgoing = jnp.dot(
-        chosen.astype(jnp.bfloat16), normal_ffn, preferred_element_type=jnp.float32
-    ).astype(jnp.bfloat16)
-    outgoing = outgoing.reshape(expert_count, slot_count, model_width)
-    arrived = lax.all_to_all(outgoing, "ep", split_axis=0, concat_axis=0, tiled=True)
-    outputs = swiglu(
-        arrived.reshape(-1, model_width), expert_gate[0], expert_up[0], expert_down[0]
-    ).astype(jnp.bfloat16)
-    returned = lax.all_to_all(
-        outputs.reshape(arrived.shape), "ep", split_axis=0, concat_axis=0, tiled=True
-    )
-    weights_by_slot = placed * route_weight.reshape(-1)[None, :]
-    combine = jnp.sum(
-        weights_by_slot.reshape(expert_count * slot_count, seq_count, top_count), axis=2
-    )
-    return lax.dot_general(
-        combine,
-        returned.reshape(-1, model_width).astype(jnp.float32),
-        (((0,), (0,)), ((), ())),
-        precision=lax.Precision.HIGHEST,
-    )
+f32 = jnp.float32
+bf16 = jnp.bfloat16
+
+
+def slice_dims(device_count):
+    side = max(1, math.isqrt(device_count // 8))
+    return device_count // (2 * side * side), side, side
+
+
+def mm(a, b):
+    return lax.dot_general(a, b, (((1,), (0,)), ((), ())), preferred_element_type=f32)
+
+
+def mm_t(a, b):
+    return lax.dot_general(a, b, (((1,), (1,)), ((), ())), preferred_element_type=f32)
+
+
+def silu(v):
+    return v / (1.0 + jnp.exp(-v))
+
+
+def channel_mixer(
+    dims,
+    width,
+    expert_count,
+    block_ref,
+    residual_ref,
+    mix_ref,
+    eg_hbm,
+    eu_hbm,
+    ed_hbm,
+    dg_hbm,
+    du_hbm,
+    dd_hbm,
+    sg_hbm,
+    su_hbm,
+    sd_hbm,
+    out_ref,
+    eg,
+    eu,
+    ed,
+    dg,
+    du,
+    dd,
+    sg,
+    su,
+    sd,
+    gathered,
+    partial,
+    in_core,
+    sum_core,
+    in2a,
+    in2b,
+    sum2a,
+    sum2b,
+    in3a,
+    in3b,
+    sum3,
+    in4,
+    total,
+    w_sem,
+    own_sem,
+    gz_s,
+    gz_r,
+    g2a_s,
+    g2a_r,
+    g2b_s,
+    g2b_r,
+    g3a_s,
+    g3a_r,
+    g3b_s,
+    g3b_r,
+    g4_s,
+    g4_r,
+    r1_s,
+    r1_r,
+    r2a_s,
+    r2a_r,
+    r2b_s,
+    r2b_r,
+    r3a_s,
+    r3a_r,
+    r3b_s,
+    r3b_r,
+    r4_s,
+    r4_r,
+):
+    zs, ys, xs = dims
+    half = width // 2
+    me = lax.axis_index("ep")
+    core = lax.rem(me, 2)
+    x = lax.rem(me // 2, xs)
+    y = lax.rem(me // (2 * xs), ys)
+    z = me // (2 * xs * ys)
+    other = 1 - core
+
+    def turn(at, by, size):
+        return lax.rem(at + by + size, size)
+
+    def device(zz, yy, xx, cc):
+        return ((zz * ys + yy) * xs + xx) * 2 + cc
+
+    def z_peer(by):
+        return device(turn(z, by, zs), y, x, core)
+
+    def y_peer(by):
+        return device(z, turn(y, by, ys), x, core)
+
+    def x_peer(by):
+        return device(z, y, turn(x, by, xs), core)
+
+    mate = device(z, y, x, other)
+    peers = (
+        [z_peer(p) for p in range(1, zs)]
+        + [y_peer(p) for p in range(1, ys)]
+        + [x_peer(p) for p in range(1, xs)]
+        + [mate]
+    )
+
+    loads = []
+    for at, (a, b) in enumerate(
+        [
+            (sg_hbm, sg),
+            (su_hbm, su),
+            (sd_hbm, sd),
+            (eg_hbm.at[0], eg),
+            (eu_hbm.at[0], eu),
+            (ed_hbm.at[0], ed),
+            (dg_hbm, dg),
+            (du_hbm, du),
+            (dd_hbm, dd),
+        ]
+    ):
+        load = pltpu.make_async_copy(a, b, w_sem.at[at])
+        load.start()
+        loads.append(load)
+    own = pltpu.make_async_copy(block_ref, gathered.at[z, y, x, core], own_sem)
+    own.start()
+
+    barrier = pltpu.get_barrier_semaphore()
+    for peer in peers:
+        pl.semaphore_signal(
+            barrier, inc=1, device_id=(peer,), device_id_type=pl.DeviceIdType.MESH
+        )
+    pl.semaphore_wait(barrier, len(peers))
+
+    started = []
+
+    def send(source, target, send_sem, recv_sem, peer):
+        copy = pltpu.make_async_remote_copy(
+            src_ref=source,
+            dst_ref=target,
+            send_sem=send_sem,
+            recv_sem=recv_sem,
+            device_id=(peer,),
+            device_id_type=pl.DeviceIdType.MESH,
+        )
+        copy.start()
+        started.append(copy)
+        return copy
+
+    own.wait()
+    for_z, for2, for3, for4 = {}, {}, {}, {}
+    for o in range(1, zs):
+        mine = gathered.at[z, y, x, core]
+        for_z[o] = send(mine, mine, gz_s.at[o - 1], gz_r.at[o - 1], z_peer(o))
+
+    def spread2(o):
+        at = turn(z, -o, zs)
+        if o:
+            for_z[o].wait_recv()
+        a = gathered.at[at, y, x, core, :, pl.ds(0, half)]
+        b = gathered.at[at, y, x, core, :, pl.ds(half, gathered.shape[-1] - half)]
+        for2[o] = [
+            send(a, a, g2a_s.at[o, p - 1], g2a_r.at[o, p - 1], y_peer(p)) for p in range(1, ys)
+        ] + [send(b, b, g2b_s.at[o, p - 1], g2b_r.at[o, p - 1], x_peer(p)) for p in range(1, xs)]
+
+    def spread3(o):
+        at = turn(z, -o, zs)
+        for copy in for2[o]:
+            copy.wait_recv()
+        a = gathered.at[at, :, x, core, :, pl.ds(0, half)]
+        b = gathered.at[at, y, :, core, :, pl.ds(half, gathered.shape[-1] - half)]
+        for3[o] = [
+            send(a, a, g3a_s.at[o, p - 1], g3a_r.at[o, p - 1], x_peer(p)) for p in range(1, xs)
+        ] + [send(b, b, g3b_s.at[o, p - 1], g3b_r.at[o, p - 1], y_peer(p)) for p in range(1, ys)]
+
+    def spread4(o):
+        at = turn(z, -o, zs)
+        for copy in for3[o]:
+            copy.wait_recv()
+        a = gathered.at[at, :, :, core]
+        for4[o] = send(a, a, g4_s.at[o], g4_r.at[o], mate)
+
+    to1, to2, to3, to4 = {}, {}, {}, {}
+    gate = 1.0 / (1.0 + jnp.exp(-mix_ref[...]))
+
+    def branches(o):
+        at = turn(z, -o, zs)
+        if o == 0:
+            for load in loads[3:]:
+                load.wait()
+        for4[o].wait_recv()
+        rows = ys * xs * 2 * gathered.shape[4]
+        block = gathered[at].reshape(rows, gathered.shape[-1])
+        inputs = block[:, :width]
+        extra = block[:, width:].astype(f32)
+        lane = lax.broadcasted_iota(jnp.int32, extra.shape, 1)
+        chosen = (lane == me) | (lane == me + expert_count)
+        weight = jnp.sum(jnp.where(chosen, extra, 0.0), axis=1, keepdims=True)
+        hidden = (silu(mm(inputs, eg[...])) * mm(inputs, eu[...])).astype(bf16)
+        dense = (silu(mm_t(inputs, dg[...])) * mm_t(inputs, du[...])).astype(bf16)
+        terms = weight * mm(hidden, ed[...]) + gate * mm(dense, dd[...])
+        partial[at] = terms.astype(bf16).reshape(partial.shape[1:])
+        to1[o] = send(
+            partial.at[at, :, :, other], in_core.at[o], r1_s.at[o], r1_r.at[o], mate
+        )
+
+    def reduce2(o):
+        at = turn(z, -o, zs)
+        to1[o].wait_recv()
+        sum_core[o] = (partial[at, :, :, core].astype(f32) + in_core[o].astype(f32)).astype(bf16)
+        to2[o] = [
+            send(
+                sum_core.at[o, :, turn(x, p, xs), :, pl.ds(0, half)],
+                in2a.at[o, p - 1],
+                r2a_s.at[o, p - 1],
+                r2a_r.at[o, p - 1],
+                x_peer(p),
+            )
+            for p in range(1, xs)
+        ] + [
+            send(
+                sum_core.at[o, turn(y, p, ys), :, :, pl.ds(half, width - half)],
+                in2b.at[o, p - 1],
+                r2b_s.at[o, p - 1],
+                r2b_r.at[o, p - 1],
+                y_peer(p),
+            )
+            for p in range(1, ys)
+        ]
+
+    def reduce3(o):
+        for copy in to2[o]:
+            copy.wait_recv()
+        a = sum_core[o, :, x, :, 0:half].astype(f32)
+        for p in range(1, xs):
+            a = a + in2a[o, p - 1].astype(f32)
+        sum2a[o] = a.astype(bf16)
+        b = sum_core[o, y, :, :, half:width].astype(f32)
+        for p in range(1, ys):
+            b = b + in2b[o, p - 1].astype(f32)
+        sum2b[o] = b.astype(bf16)
+        to3[o] = [
+            send(
+                sum2a.at[o, turn(y, p, ys)],
+                in3a.at[o, p - 1],
+                r3a_s.at[o, p - 1],
+                r3a_r.at[o, p - 1],
+                y_peer(p),
+            )
+            for p in range(1, ys)
+        ] + [
+            send(
+                sum2b.at[o, turn(x, p, xs)],
+                in3b.at[o, p - 1],
+                r3b_s.at[o, p - 1],
+                r3b_r.at[o, p - 1],
+                x_peer(p),
+            )
+            for p in range(1, xs)
+        ]
+
+    def reduce4(o):
+        for copy in to3[o]:
+            copy.wait_recv()
+        a = sum2a[o, y].astype(f32)
+        for p in range(1, ys):
+            a = a + in3a[o, p - 1].astype(f32)
+        b = sum2b[o, x].astype(f32)
+        for p in range(1, xs):
+            b = b + in3b[o, p - 1].astype(f32)
+        if o == 0:
+            total[:, 0:half] = total[:, 0:half] + a
+            total[:, half:width] = total[:, half:width] + b
+        else:
+            sum3[o - 1, :, 0:half] = a.astype(bf16)
+            sum3[o - 1, :, half:width] = b.astype(bf16)
+            to4[o] = send(
+                sum3.at[o - 1], in4.at[o - 1], r4_s.at[o - 1], r4_r.at[o - 1], z_peer(-o)
+            )
+
+    def shared():
+        for load in loads[:3]:
+            load.wait()
+        inputs = block_ref[:, :width]
+        hidden = (silu(mm(inputs, sg[...])) * mm(inputs, su[...])).astype(bf16)
+        total[...] = mm(hidden, sd[...])
+
+    stages = [spread2, spread3, spread4, branches, reduce2, reduce3, reduce4]
+    for step in range(zs + len(stages) - 1):
+        for at, stage in enumerate(stages):
+            if 0 <= step - at < zs:
+                stage(step - at)
+        if step == 0:
+            shared()
+
+    combined = total[...]
+    for o in range(1, zs):
+        to4[o].wait_recv()
+        combined = combined + in4[o - 1].astype(f32)
+    scale = lax.rsqrt(jnp.mean(combined * combined, axis=-1, keepdims=True) + eps)
+    out_ref[...] = (residual_ref[...] + combined * scale).astype(bf16)
+    for copy in started:
+        copy.wait_send()
+
+
+def mixed_channels(block, residual, dense_mix, weights, expert_count, device_count):
+    seq_count, width = residual.shape
+    wide = block.shape[1]
+    zs, ys, xs = slice_dims(device_count)
+    half = width // 2
+    rest = width - half
+    y1, x1, z1 = max(ys - 1, 1), max(xs - 1, 1), max(zs - 1, 1)
+    held = [pltpu.VMEM(w.shape[-2:], bf16) for w in weights]
+    dma = pltpu.SemaphoreType.DMA
+    buffers = [
+        pltpu.VMEM((zs, ys, xs, 2, seq_count, wide), bf16),
+        pltpu.VMEM((zs, ys, xs, 2, seq_count, width), bf16),
+        pltpu.VMEM((zs, ys, xs, seq_count, width), bf16),
+        pltpu.VMEM((zs, ys, xs, seq_count, width), bf16),
+        pltpu.VMEM((zs, x1, ys, seq_count, half), bf16),
+        pltpu.VMEM((zs, y1, xs, seq_count, rest), bf16),
+        pltpu.VMEM((zs, ys, seq_count, half), bf16),
+        pltpu.VMEM((zs, xs, seq_count, rest), bf16),
+        pltpu.VMEM((zs, y1, seq_count, half), bf16),
+        pltpu.VMEM((zs, x1, seq_count, rest), bf16),
+        pltpu.VMEM((z1, seq_count, width), bf16),
+        pltpu.VMEM((z1, seq_count, width), bf16),
+        pltpu.VMEM((seq_count, width), f32),
+    ]
+    sems = [dma((len(weights),)), dma]
+    for shape in [
+        (z1,),
+        (zs, y1),
+        (zs, x1),
+        (zs, x1),
+        (zs, y1),
+        (zs,),
+        (zs,),
+        (zs, x1),
+        (zs, y1),
+        (zs, y1),
+        (zs, x1),
+        (z1,),
+    ]:
+        sems += [dma(shape), dma(shape)]
+    vmem = pl.BlockSpec(memory_space=pltpu.VMEM)
+    return pl.pallas_call(
+        functools.partial(channel_mixer, (zs, ys, xs), width, expert_count),
+        out_shape=jax.ShapeDtypeStruct((seq_count, width), bf16),
+        in_specs=[vmem] * 3 + [pl.BlockSpec(memory_space=pl.ANY)] * len(weights),
+        out_specs=vmem,
+        scratch_shapes=held + buffers + sems,
+        compiler_params=pltpu.CompilerParams(
+            collective_id=0, has_side_effects=True, vmem_limit_bytes=56 * 1024 * 1024
+        ),
+    )(block, residual, dense_mix.reshape(1, width), *weights)
 
 
 def per_device(
@@ -196,21 +501,34 @@
         retention_state,
     )
     normal_ffn = (normed(residual) * ffn_gain).astype(jnp.bfloat16)
-    seq_count, top_count = routes.shape
-    shared_out = swiglu(normal_ffn, shared_gate, shared_up, shared_down)
-    gated = jax.nn.sigmoid(dense_mix)
+    device_count = lax.axis_size("ep")
+    expert_count = device_count * expert_gate.shape[0]
     route_weight = route_scores / jnp.sum(route_scores, axis=-1, keepdims=True) * route_scale
-    gathered = gather_tokens(normal_ffn)
-
-    def dense_rows(row_start, row_count):
-        return gated * dense_part(gathered, dense_gate, dense_up, dense_down)
-
-    combined = (
-        shared_out
-        + branch_sums(dense_rows, seq_count)
-        + exchanged_experts(normal_ffn, routes, route_weight, expert_gate, expert_up, expert_down)
-    )
-    layer_out = (residual + normed(combined)).astype(jnp.bfloat16)
+    named = routes[:, :, None] == jnp.arange(expert_count, dtype=jnp.int32)[None, None, :]
+    by_expert = jnp.sum(jnp.where(named, route_weight[:, :, None], 0.0), axis=1)
+    upper = lax.reduce_precision(by_expert, 8, 7)
+    pad = -(2 * expert_count) % 128
+    block = jnp.concatenate(
+        [
+            normal_ffn,
+            upper.astype(bf16),
+            (by_expert - upper).astype(bf16),
+            jnp.zeros((routes.shape[0], pad), bf16),
+        ],
+        axis=1,
+    )
+    weights = (
+        expert_gate,
+        expert_up,
+        expert_down,
+        dense_gate,
+        dense_up,
+        dense_down,
+        shared_gate,
+        shared_up,
+        shared_down,
+    )
+    layer_out = mixed_channels(block, residual, dense_mix, weights, expert_count, device_count)
     return (layer_out, new_keys, new_values)
 
 

time: 240 us -> 61.9 us (0.26)
  waiting for transfers between devices: 165 us -> 0 us
  Pallas kernels: 0 us -> 35.2 us
  blocking collectives: 20.1 us -> 0 us
  between operations: 14.3 us -> 0.87 us
  matrix products: 26.3 us -> 15.4 us
  starting transfers between devices: 2.96 us -> 0 us
    reduce_scatter x1 -> x0, waiting for transfers between devices: 109 us -> none  [branch_sums(): lax.psum_scatter(term_rows(jnp.int32(0), seq_count * lax.axis_size('ep'))...]
    all_gather x1 -> x0, waiting for transfers between devices: 56.4 us -> none  [gather_tokens(): return lax.all_gather(normal_ffn, 'ep', axis=0, tiled=True)]
    pallas_call x0 -> x1, Pallas kernels: none -> 35.2 us  [mixed_channels(): pl.pallas_call(functools.partial(channel_mixer, (zs, ys, xs), width, expe...]
    all_to_all x1 -> x0, blocking collectives: 20.1 us -> none  [exchanged_experts(): lax.all_to_all(outgoing, 'ep', split_axis=0, concat_axis=0, tiled=True)]
    dot_general x8 -> x0, matrix products: 13.1 us -> none  [the longest x2 4.41 us: swiglu(): return jnp.dot(hidden, w_down, preferred_element_type=jnp.float32)]
    all_to_all x1 -> x0, starting transfers between devices: 2.88 us -> none  [exchanged_experts(): lax.all_to_all(outputs.reshape(arrived.shape), 'ep', split_axis=0, concat...]
  transfers between devices with their start and end apart: 3 -> 0, of which waited for: 2 -> 0; matrix products, arithmetic and copies ran while one was open for 4% -> 0% of each run, Pallas kernels for 0% -> 0%
where the time goes in v1:
time: 61.9 us; the launch traced here: 61.4 us
  Pallas kernels  35.2 us (57%)
  matrix products  15.4 us (25%)
  local copies, waits for them, and re-layouts  6.74 us (11%)
  other arithmetic  3.24 us (5%)
  between operations  0.87 us (1%)
    pallas_call x1, Pallas kernels, mixed_channels(): pl.pallas_call(functools.partial(channel_mixer, (zs, ys, xs), width, expe...  35.2 us
    dot_general x1, matrix products, retain(): jnp.einsum('shd,shde->she', queries.astype(jnp.float32), carry_state, pre...  6.26 us
    reshape x1, local copies, waits for them, and re-layouts, retain(): cache_keys.reshape(seq_count, block_size, head_count, key_size)  3.93 us
    dot_general x1, matrix products, retain(): jnp.einsum('shj,sjhe->she', weighted, stored_values, preferred_element_ty...  2.84 us
    dot_general x1, matrix products, retain(): jnp.einsum('shd,sjhd->shj', queries, stored_keys, preferred_element_type=...  2.24 us
    unnamed x23, local copies, waits for them, and re-layouts  2.04 us
    dot_general x1, matrix products, retain(): jnp.dot(normal_in, w_query, preferred_element_type=jnp.float32)  1.55 us
    dot_general x1, matrix products, retain(): jnp.dot(normal_in, w_key, preferred_element_type=jnp.float32)  1.55 us

profile of v1, /device:TPU:0, one launch (start us, length us, event | category | flops | bytes accessed | tf_op | source)
XLA Modules:
  0.0 61.4 jit_solution(16598637189115214346)
XLA Ops:
  0.6 0.0 copy-start
  0.6 1.0 %fusion.3 = f32[16]{0:T(128)S(1)} fusion(bf16[16,1024]{1,0:T(8,128)(2,1)} %param.23), kind=kLoop, calls=%fused_computation.7 | loop fusion | flops 49136 | bytes 32832 | tf_op jit(solution)/shard_map/reduce_sum | solution.py:17
  1.7 1.6 %fusion.19 = f32[16,512]{1,0:T(8,128)S(1)} fusion(bf16[1024,512]{1,0:T(8,128)(2,1)} %param.29, bf16[16,1024]{1,0:T(8,128)(2,1)} %param.23, f32[1024]{0:T(1024)} %param.28, f32[16]{0:T(128)S(1)} %add_rsqrt_fusion.3), kind=kOutput, calls=%fused_computation.58 | convolution fusion | flops 16842752 | bytes 1118272 | tf_op jit(solution)/shard_map/dot_general | solution.py:45
  3.3 0.7 %convert_element_type.79 = f32[16]{0:T(128)S(1)} convert(s32[16]{0:T(128)} %param.24) | non-fusion elementwise | flops 16 | bytes 128 | tf_op jit(solution)/shard_map/convert_element_type | solution.py:27
  3.9 0.1 multiply_cosine_fusion
  4.1 0.1 multiply_subtract_fusion.1
  4.1 1.5 %fusion.17 = f32[16,512]{1,0:T(8,128)S(1)} fusion(bf16[1024,512]{1,0:T(8,128)(2,1)} %param.30, bf16[16,1024]{1,0:T(8,128)(2,1)} %param.23, f32[1024]{0:T(1024)} %param.28, f32[16]{0:T(128)S(1)} %add_rsqrt_fusion.3), kind=kOutput, calls=%fused_computation.57 | convolution fusion | flops 16842752 | bytes 1118272 | tf_op jit(solution)/shard_map/dot_general | solution.py:48
  5.7 0.1 multiply_subtract_fusion
  5.8 0.2 multiply_reduce_fusion.3
  6.0 3.9 %copy.35 = bf16[16,128,512]{1,2,0:T(8,128)(2,1)} copy(bf16[16,128,512]{2,1,0:T(8,128)(2,1)} %param.25) | data formatting | bytes 4194304 | tf_op jit(solution)/shard_map/reshape | solution.py:60
  9.9 0.0 copy-start.9
  9.9 2.2 %fusion.11 = f32[16,4,1,128]{3,2,1,0:T(1,128)S(1)} fusion(bf16[16,128,4,128]{1,3,2,0:T(8,128)(2,1)} %bitcast.34, bf16[16,4,128,1]{2,1,0,3:T(4,128)(2,1)S(1)} %bitcast.36), kind=kOutput, calls=%fused_computation.32 | convolution fusion | flops 2097152 | bytes 2146304 | tf_op jit(solution)/shard_map/shd,sjhd->shj/dot_general | solution.py:62
  12.2 0.0 copy-done.9
  12.2 0.1 maximum_convert_fusion.1
  12.3 0.1 iota_compare_fusion.1
  12.4 0.1 fusion.13
  12.5 2.8 %fusion = f32[16,4,1,256]{3,2,1,0:T(1,128)S(1)} fusion(bf16[16,16,4,8,256]{4,3,2,1,0:T(8,128)(2,1)} %bitcast.35, bf16[16,4,128,1]{2,1,0,3:T(4,128)(2,1)S(1)} %fusion.13), kind=kOutput, calls=%fused_computation | convolution fusion | flops 4194304 | bytes 4276224 | tf_op jit(solution)/shard_map/shj,sjhe->she/dot_general | solution.py:73
  15.3 0.0 copy-start.1
  15.3 0.0 copy-start.2
  15.3 0.0 copy-start.5
  15.3 6.3 %fusion.9 = f32[16,4,1,256]{3,2,1,0:T(1,128)S(1)} fusion(f32[16,4,128,256]{3,2,1,0:T(8,128)} %param.27, bf16[16,4,128,1]{2,1,0,3:T(4,128)(2,1)S(1)} %bitcast.37), kind=kOutput, calls=%fused_computation.30 | convolution fusion | flops 25165824 | bytes 8470528 | tf_op jit(solution)/shard_map/shd,shde->she/dot_general | solution.py:77
  21.6 0.0 copy-done.1
  21.6 0.0 copy-done.2
  21.6 0.0 copy-done.5
  21.6 0.0 copy-start.7
  21.6 0.0 copy-start.6
  21.6 0.0 copy-start.8
  21.7 0.4 convolution_convert_fusion
  22.1 0.0 copy-start.4
  22.1 0.1 multiply_exponential_fusion
  22.2 0.2 multiply_reduce_fusion.2
  22.4 0.1 multiply_convert_fusion.1
  22.5 0.0 copy-done
  22.5 0.5 multiply_reduce_fusion.1
  23.0 0.2 multiply_reduce_fusion
  23.2 0.0 copy-start.3
  23.3 0.0 copy-done.7
  23.3 0.1 multiply_convert_fusion
  23.3 0.0 copy-done.6
  23.4 0.0 copy-done.8
  23.4 0.1 select_reduce_fusion
  23.5 0.7 %concatenate.11.block_ref = bf16[16,1152]{1,0:T(8,128)(2,1)} concatenate(bf16[16,1024]{1,0:T(8,128)(2,1)S(1)} %multiply_convert_fusion, bf16[16,32]{1,0:T(8,128)(2,1)S(1)} %get-tuple-element.17, bf16[16,32]{1,0:T(8,128)(2,1)S(1)} %get-tuple-element.16, bf16[16,64]{1,0:T(8,128)(2,1)S(1)} %broadcast_in_dim.26), dimensions={1} | concatenate | bytes 73728 | tf_op jit(solution)/shard_map/concatenate | solution.py:511
  24.2 0.0 copy-done.3
  24.2 35.2 %shard_map.238 = bf16[16,1024]{1,0:T(8,128)(2,1)} custom-call(bf16[16,1152]{1,0:T(8,128)(2,1)} %concatenate.11.block_ref, f32[16,1024]{1,0:T(8,128)} %copy-done.3, f32[1,1024]{1,0:T(1,128)} %bitcast.43, bf16[1,1024,256]{2,1,0:T(8,128)(2,1)} %eg_hbm.1, bf16[1,1024,256]{2,1,0:T(8,128)(2,1)} %eu_hbm.1, bf16[1,256,1024]{2,1,0:T(8,128)(2,1)} %ed_hbm.1, ...), custom_call_target="tpu_custom_call" | custom-call | tf_op jit(solution)/shard_map/pallas_call | solution.py:454
  59.4 0.0 copy-done.4
  59.4 0.6 copy.54
  60.1 1.4 %copy.56 = bf16[16,1024]{1,0:T(8,128)(2,1)} copy(bf16[16,1024]{1,0:T(8,128)(2,1)} %shard_map.238) | data formatting | bytes 65536
  (16 shorter events, 0.2 us)
Async XLA Ops:
  0.6 21.9 %copy-start = (bf16[1024,1024]{1,0:T(8,128)(2,1)S(1)}, bf16[1024,1024]{1,0:T(8,128)(2,1)}, u32[]{:S(2)}) copy-start(bf16[1024,1024]{1,0:T(8,128)(2,1)} %param.32) | copy-start | bytes 6291460
  9.9 2.2 %copy-start.9 = (s32[16]{0:T(128)S(1)}, s32[16]{0:T(128)}, u32[]{:S(2)}) copy-start(s32[16]{0:T(128)} %param.24) | copy-start | bytes 196
  15.3 6.3 %copy-start.1 = (bf16[1024,1024]{1,0:T(8,128)(2,1)S(1)}, bf16[1024,1024]{1,0:T(8,128)(2,1)}, u32[]{:S(2)}) copy-start(bf16[1024,1024]{1,0:T(8,128)(2,1)} %param.31) | copy-start | bytes 6291460
  15.3 6.3 %copy-start.2 = (bf16[16,1024]{1,0:T(8,128)(2,1)S(1)}, bf16[16,1024]{1,0:T(8,128)(2,1)}, u32[]{:S(2)}) copy-start(bf16[16,1024]{1,0:T(8,128)(2,1)} %param.23) | copy-start | bytes 98308
  15.3 6.3 %copy-start.5 = (f32[1024]{0:T(1024)S(1)}, f32[1024]{0:T(1024)}, u32[]{:S(2)}) copy-start(f32[1024]{0:T(1024)} %param.28) | copy-start | bytes 12292
  21.6 1.6 %copy-start.7 = (f32[1024]{0:T(1024)S(1)}, f32[1024]{0:T(1024)}, u32[]{:S(2)}) copy-start(f32[1024]{0:T(1024)} %param.33) | copy-start | bytes 12292
  21.6 1.7 %copy-start.6 = (f32[16,6]{0,1:T(8,128)S(1)}, f32[16,6]{0,1:T(8,128)}, u32[]{:S(2)}) copy-start(f32[16,6]{0,1:T(8,128)} %param.35) | copy-start | bytes 1156
  21.6 1.7 %copy-start.8 = (s32[16,6]{0,1:T(8,128)S(1)}, s32[16,6]{0,1:T(8,128)}, u32[]{:S(2)}) copy-start(s32[16,6]{0,1:T(8,128)} %param.34) | copy-start | bytes 1156
  22.1 37.4 %copy-start.4 = (bf16[16,1024]{1,0:T(8,128)(2,1)}, bf16[16,1024]{1,0:T(8,128)(2,1)S(1)}, u32[]{:S(2)}) copy-start(bf16[16,1024]{1,0:T(8,128)(2,1)S(1)} %convolution_convert_fusion) | copy-start | bytes 98308
  23.2 1.0 %copy-start.3 = (f32[16,1024]{1,0:T(8,128)}, f32[16,1024]{1,0:T(8,128)S(1)}, u32[]{:S(2)}) copy-start(f32[16,1024]{1,0:T(8,128)S(1)} %get-tuple-element.4.residual_ref) | copy-start | bytes 196612

commit v2 on v1

--- a/solution.py
+++ b/solution.py
@@ -35,6 +35,57 @@
     )
 
 
+f32 = jnp.float32
+bf16 = jnp.bfloat16
+
+
+def slice_dims(device_count):
+    side = max(1, math.isqrt(device_count // 8))
+    return device_count // (2 * side * side), side, side
+
+
+def mm(a, b):
+    return lax.dot_general(a, b, (((1,), (0,)), ((), ())), preferred_element_type=f32)
+
+
+def mm_t(a, b):
+    return lax.dot_general(a, b, (((1,), (1,)), ((), ())), preferred_element_type=f32)
+
+
+def block_reads(query_ref, column_ref, decay_ref, key_ref, value_ref, state_ref, out_ref):
+    head_count, value_size = state_ref.shape[1], state_ref.shape[3]
+    for at in range(key_ref.shape[0]):
+        scores = mm_t(query_ref[at], key_ref[at])
+        cross = mm((scores * decay_ref[at]).astype(bf16), value_ref[at])
+        row = lax.broadcasted_iota(jnp.int32, cross.shape, 0) * value_size
+        lane = lax.broadcasted_iota(jnp.int32, cross.shape, 1)
+        own_head = (lane >= row) & (lane < row + value_size)
+        inside = jnp.sum(jnp.where(own_head, cross, 0.0), axis=0, keepdims=True)
+        columns = column_ref[at]
+        carried = [
+            jnp.sum(columns[:, h : h + 1] * state_ref[at, h], axis=0, keepdims=True)
+            for h in range(head_count)
+        ]
+        out_ref[at] = inside + jnp.concatenate(carried, axis=1)
+
+
+def read_blocks(spread, columns, decay, cache_keys, cache_values, carry_state):
+    operands = (spread, columns, decay, cache_keys, cache_values, carry_state)
+    seq_count, width = cache_values.shape[0], cache_values.shape[2]
+    step = 2 if seq_count % 2 == 0 else 1
+
+    def rows(shape):
+        return pl.BlockSpec((step,) + shape[1:], lambda i: (i,) + (0,) * (len(shape) - 1))
+
+    return pl.pallas_call(
+        block_reads,
+        grid=(seq_count // step,),
+        out_shape=jax.ShapeDtypeStruct((seq_count, 1, width), f32),
+        in_specs=[rows(a.shape) for a in operands],
+        out_specs=rows((seq_count, 1, width)),
+    )(*operands)
+
+
 def retain(
     tokens, lengths, mix_gain, w_query, w_key, w_value, w_out, cache_keys, cache_values, carry_state
 ):
@@ -57,32 +108,28 @@
     filled = lengths % block_size
     decay_rate = log_decay(head_count)
     places = jnp.arange(block_size, dtype=jnp.int32)
-    stored_keys = cache_keys.reshape(seq_count, block_size, head_count, key_size)
-    stored_values = cache_values.reshape(seq_count, block_size, head_count, value_size)
-    scores = jnp.einsum("shd,sjhd->shj", queries, stored_keys, preferred_element_type=jnp.float32)
     distance = jnp.maximum(filled[:, None] - places[None, :], 0).astype(jnp.float32)
     live_mask = places[None, :] < filled[:, None]
-    weighted = jnp.where(
-        live_mask[:, None, :],
-        scores * jnp.exp(distance[:, None, :] * decay_rate[None, :, None]),
-        0.0,
-    ).astype(jnp.bfloat16)
+    head_rows = -(-head_count // 16) * 16
+    row_rate = jnp.concatenate([decay_rate, jnp.zeros((head_rows - head_count,), jnp.float32)])
+    decay = jnp.where(
+        live_mask[:, None, :], jnp.exp(distance[:, None, :] * row_rate[None, :, None]), 0.0
+    )
+    same_head = jnp.arange(head_rows)[:, None] == jnp.arange(head_count)[None, :]
+    spread = jnp.where(same_head[None, :, :, None], queries[:, None], 0).reshape(
+        seq_count, head_rows, head_count * key_size
+    )
+    carry_scale = jnp.exp((filled.astype(jnp.float32)[:, None] + 1.0) * decay_rate[None, :])
+    scaled = queries.astype(jnp.float32) * carry_scale[:, :, None]
+    columns = jnp.swapaxes(scaled, 1, 2)
     own_weight = jnp.sum(
         queries.astype(jnp.float32) * new_keys.astype(jnp.float32), axis=-1
     ).astype(jnp.bfloat16)
-    inside = jnp.einsum(
-        "shj,sjhe->she", weighted, stored_values, preferred_element_type=jnp.float32
-    )
+    inside = read_blocks(spread, columns, decay, cache_keys, cache_values, carry_state)
+    inside = inside.reshape(seq_count, head_count, value_size)
     inside = inside + own_weight.astype(jnp.float32)[:, :, None] * new_values.astype(jnp.float32)
-    carried = jnp.einsum(
-        "shd,shde->she", queries.astype(jnp.float32), carry_state, precision=lax.Precision.HIGHEST
-    )
-    carried = (
-        carried
-        * jnp.exp((filled.astype(jnp.float32)[:, None] + 1.0) * decay_rate[None, :])[:, :, None]
-    )
     headed = (
-        normed(inside + carried).astype(jnp.bfloat16).reshape(seq_count, head_count * value_size)
+        normed(inside).astype(jnp.bfloat16).reshape(seq_count, head_count * value_size)
     )
     mixer_out = jnp.dot(headed, w_out, preferred_element_type=jnp.float32)
     residual = widened + normed(mixer_out)
@@ -91,23 +138,6 @@
         new_keys.reshape(seq_count, head_count * key_size),
         new_values.reshape(seq_count, head_count * value_size),
     )
-
-
-f32 = jnp.float32
-bf16 = jnp.bfloat16
-
-
-def slice_dims(device_count):
-    side = max(1, math.isqrt(device_count // 8))
-    return device_count // (2 * side * side), side, side
-
-
-def mm(a, b):
-    return lax.dot_general(a, b, (((1,), (0,)), ((), ())), preferred_element_type=f32)
-
-
-def mm_t(a, b):
-    return lax.dot_general(a, b, (((1,), (1,)), ((), ())), preferred_element_type=f32)
 
 
 def silu(v):

time: 61.9 us -> 62.3 us (level)
  matrix products: 15.4 us -> 5.61 us
  Pallas kernels: 35.2 us -> 44.9 us
  other arithmetic: 3.24 us -> 5.58 us
  local copies, waits for them, and re-layouts: 6.74 us -> 4.84 us
    dot_general x3 -> x0, matrix products: 11.3 us -> none  [the longest x1 6.26 us: retain(): jnp.einsum('shd,shde->she', queries.astype(jnp.float32), carry_state, pre...]
    pallas_call x0 -> x1, Pallas kernels: none -> 9.64 us  [read_blocks(): pl.pallas_call(block_reads, grid=(seq_count // step,), out_shape=jax.Shap...]
    reshape x1, local copies, waits for them, and re-layouts: 3.93 us -> 0.03 us  [retain(): inside = inside.reshape(seq_count, head_count, value_size)]
    dot_general x1, matrix products: 0.42 us -> 2.01 us  [retain(): jnp.dot(normal_in, w_value, preferred_element_type=jnp.float32)]
    mul x0 -> x3, local copies, waits for them, and re-layouts: none -> 1.54 us  [the longest x1 1.38 us: retain(): scaled = queries.astype(jnp.float32) * carry_scale[:, :, None]]
    select_n x0 -> x2, other arithmetic: none -> 1.49 us  [the longest x1 0.74 us: retain(): jnp.where(same_head[None, :, :, None], queries[:, None], 0)]
    pallas_call x0 -> x1, other arithmetic: none -> 1.06 us  [read_blocks(): pl.pallas_call(block_reads, grid=(seq_count // step,), out_shape=jax.Shap...]
    convert_element_type x0 -> x3, local copies, waits for them, and re-layouts: none -> 0.71 us  [the longest x1 0.61 us: retain(): new_keys = rotate(raw_key, lengths).astype(jnp.bfloat16)]
where the time goes in v2:
time: 62.3 us; the launch traced here: 61.8 us
  Pallas kernels  44.9 us (72%)
  matrix products  5.61 us (9%)
  other arithmetic  5.58 us (9%)
  local copies, waits for them, and re-layouts  4.84 us (8%)
  between operations  0.92 us (1%)
    pallas_call x1, Pallas kernels, mixed_channels(): pl.pallas_call(functools.partial(channel_mixer, (zs, ys, xs), width, expe...  35.2 us
    pallas_call x1, Pallas kernels, read_blocks(): pl.pallas_call(block_reads, grid=(seq_count // step,), out_shape=jax.Shap...  9.64 us
    dot_general x1, matrix products, retain(): jnp.dot(normal_in, w_value, preferred_element_type=jnp.float32)  2.01 us
    dot_general x1, matrix products, retain(): jnp.dot(normal_in, w_query, preferred_element_type=jnp.float32)  1.55 us
    unnamed x26, local copies, waits for them, and re-layouts  1.55 us
    dot_general x1, matrix products, retain(): jnp.dot(normal_in, w_key, preferred_element_type=jnp.float32)  1.55 us
    reduce_sum x3, other arithmetic, normed(): jnp.mean(values * values, axis=-1, keepdims=True) + eps  1.39 us
    mul x1, local copies, waits for them, and re-layouts, retain(): scaled = queries.astype(jnp.float32) * carry_scale[:, :, None]  1.38 us

profile of v2, /device:TPU:0, one launch (start us, length us, event | category | flops | bytes accessed | tf_op | source)
XLA Modules:
  0.0 61.8 jit_solution(6965447461064108117)
XLA Ops:
  0.6 0.0 copy-start
  0.6 0.0 copy-start.9
  0.7 1.0 %fusion = f32[16]{0:T(128)S(1)} fusion(bf16[16,1024]{1,0:T(8,128)(2,1)} %param.23), kind=kLoop, calls=%fused_computation.6 | loop fusion | flops 49136 | bytes 32832 | tf_op jit(solution)/shard_map/reduce_sum | solution.py:17
  1.7 1.6 %fusion.16 = f32[16,512]{1,0:T(8,128)S(1)} fusion(bf16[1024,512]{1,0:T(8,128)(2,1)} %param.29, bf16[16,1024]{1,0:T(8,128)(2,1)} %param.23, f32[1024]{0:T(1024)} %param.28, f32[16]{0:T(128)S(1)} %add_rsqrt_fusion.3), kind=kOutput, calls=%fused_computation.58 | convolution fusion | flops 16842752 | bytes 1118272 | tf_op jit(solution)/shard_map/dot_general | solution.py:96
  3.3 0.1 fusion.20
  3.4 0.7 %convert_element_type.100 = f32[16]{0:T(128)S(1)} convert(s32[16]{0:T(128)} %param.24) | non-fusion elementwise | flops 16 | bytes 128 | tf_op jit(solution)/shard_map/convert_element_type | solution.py:27
  4.0 0.1 multiply_cosine_fusion
  4.2 1.5 %fusion.14 = f32[16,512]{1,0:T(8,128)S(1)} fusion(bf16[1024,512]{1,0:T(8,128)(2,1)} %param.30, bf16[16,1024]{1,0:T(8,128)(2,1)} %param.23, f32[1024]{0:T(1024)} %param.28, f32[16]{0:T(128)S(1)} %add_rsqrt_fusion.3), kind=kOutput, calls=%fused_computation.57 | convolution fusion | flops 16842752 | bytes 1118272 | tf_op jit(solution)/shard_map/dot_general | solution.py:99
  5.7 0.1 fusion.19
  5.9 0.2 fusion.5
  6.0 0.0 copy-done.9
  6.1 0.1 multiply_exponential_fusion
  6.1 0.1 copy.96
  6.2 0.1 convert_multiply_fusion.3
  6.3 1.4 %copy.86 = f32[16,4,128]{1,2,0:T(8,128)} copy(f32[16,4,128]{2,0,1:T(8,128)S(1)} %convert_multiply_fusion.3) | data formatting | bytes 65536 | tf_op jit(solution)/shard_map/mul | solution.py:123
  7.7 0.1 fusion.8
  7.8 0.1 broadcast_in_dim.46
  7.9 0.7 %broadcast_select_fusion.query_ref = bf16[16,16,512]{2,1,0:T(8,128)(2,1)} fusion(pred[16,512]{1,0:T(8,128)(4,1)S(1)} %bitcast.45, bf16[16,512]{1,0:T(8,128)(2,1)S(1)} %bitcast.43), kind=kLoop, calls=%fused_computation.1 | loop fusion | flops 131072 | bytes 286720 | tf_op jit(solution)/shard_map/jit(_where)/select_n | solution.py:119
  8.7 0.1 maximum_convert_fusion.1
  8.7 0.1 iota_compare_fusion.1
  8.8 0.7 %exponential_select_fusion.decay_ref = f32[16,16,128]{2,1,0:T(8,128)} fusion(f32[16]{0:T(128)S(1)} %concatenate.25, f32[16,128]{1,0:T(8,128)S(1)} %maximum_convert_fusion.1, pred[16,128]{1,0:T(8,128)(4,1)S(1)} %iota_compare_fusion.1), kind=kLoop, calls=%fused_computation.2 | loop fusion | flops 65536 | bytes 141376 | tf_op jit(solution)/shard_map/jit(_where)/select_n | solution.py:115
  9.6 0.0 copy-start.1
  9.6 0.0 copy-start.5
  9.6 9.6 %shard_map.238 = f32[16,1,1024]{2,1,0:T(1,128)} custom-call(bf16[16,16,512]{2,1,0:T(8,128)(2,1)} %broadcast_select_fusion.query_ref, f32[16,128,4]{2,1,0:T(8,128)} %bitcast.36, f32[16,16,128]{2,1,0:T(8,128)} %exponential_select_fusion.decay_ref, bf16[16,128,512]{2,1,0:T(8,128)(2,1)} %key_ref.1, bf16[16,128,1024]{2,1,0:T(8,128)(2,1)} %value_ref.1, ...), custom_call_target="tpu_custom_call" | custom-call | tf_op jit(solution)/shard_map/pallas_call | solution.py:80
  19.2 0.0 copy-start.3
  19.2 1.1 %reduce = f32[16,1024]{1,0:T(8,128)S(1)} reduce(f32[16,1,1024]{2,1,0:T(1,128)} %shard_map.238, f32[]{:T(128)} %constant.61), dimensions={1}, to_apply=%pallas_call.6.reduce_sub_computation | reduce | bytes 131076 | tf_op jit(solution)/shard_map/pallas_call | solution.py:80
  20.3 0.1 copy.89
  20.4 0.0 copy-done.1
  20.4 0.0 copy-done.5
  20.4 2.0 %convolution_convert_fusion = bf16[16,1024]{1,0:T(8,128)(2,1)S(1)} fusion(bf16[1024,1024]{1,0:T(8,128)(2,1)} %param.31, bf16[16,1024]{1,0:T(8,128)(2,1)S(1)} %copy-done.1, f32[1024]{0:T(1024)S(1)} %copy-done.5, f32[16]{0:T(128)S(1)} %add_rsqrt_fusion.3), kind=kOutput, calls=%fused_computation | convolution fusion | flops 33636352 | bytes 2166848 | tf_op jit(solution)/shard_map/dot_general | solution.py:102
  22.4 0.0 copy-start.4
  22.4 0.0 copy-start.7
  22.4 0.0 copy-start.6
  22.4 0.0 copy-start.8
  22.5 0.2 multiply_reduce_fusion.2
  22.7 0.1 mul.262
  22.8 0.1 mul.257
  22.9 0.0 copy-done
  22.9 0.0 copy-done.3
  22.9 0.5 multiply_reduce_fusion.1
  23.4 0.2 multiply_reduce_fusion
  23.6 0.0 copy-start.2
  23.6 0.0 copy-done.7
  23.6 0.1 multiply_convert_fusion
  23.7 0.0 copy-done.6
  23.8 0.0 copy-done.8
  23.8 0.1 select_reduce_fusion
  23.9 0.7 %concatenate.27.block_ref = bf16[16,1152]{1,0:T(8,128)(2,1)} concatenate(bf16[16,1024]{1,0:T(8,128)(2,1)S(1)} %multiply_convert_fusion, bf16[16,32]{1,0:T(8,128)(2,1)S(1)} %get-tuple-element.19, bf16[16,32]{1,0:T(8,128)(2,1)S(1)} %get-tuple-element.18, bf16[16,64]{1,0:T(8,128)(2,1)S(1)} %broadcast_in_dim.55), dimensions={1} | concatenate | bytes 73728 | tf_op jit(solution)/shard_map/concatenate | solution.py:541
  24.6 0.0 copy-done.2
  24.6 35.2 %shard_map.239 = bf16[16,1024]{1,0:T(8,128)(2,1)} custom-call(bf16[16,1152]{1,0:T(8,128)(2,1)} %concatenate.27.block_ref, f32[16,1024]{1,0:T(8,128)} %copy-done.2, f32[1,1024]{1,0:T(1,128)} %bitcast.47, bf16[1,1024,256]{2,1,0:T(8,128)(2,1)} %eg_hbm.1, bf16[1,1024,256]{2,1,0:T(8,128)(2,1)} %eu_hbm.1, bf16[1,256,1024]{2,1,0:T(8,128)(2,1)} %ed_hbm.1, ...), custom_call_target="tpu_custom_call" | custom-call | tf_op jit(solution)/shard_map/pallas_call | solution.py:484
  59.8 0.0 copy-done.4
  59.8 0.6 copy_bitcast_fusion.2
  60.4 1.4 %copy.120 = bf16[16,1024]{1,0:T(8,128)(2,1)} copy(bf16[16,1024]{1,0:T(8,128)(2,1)} %shard_map.239) | data formatting | bytes 65536
  (24 shorter events, 0.3 us)
Async XLA Ops:
  0.6 22.3 %copy-start = (bf16[1024,1024]{1,0:T(8,128)(2,1)S(1)}, bf16[1024,1024]{1,0:T(8,128)(2,1)}, u32[]{:S(2)}) copy-start(bf16[1024,1024]{1,0:T(8,128)(2,1)} %param.32) | copy-start | bytes 6291460
  0.6 5.4 %copy-start.9 = (s32[16]{0:T(128)S(1)}, s32[16]{0:T(128)}, u32[]{:S(2)}) copy-start(s32[16]{0:T(128)} %param.24) | copy-start | bytes 196
  9.6 10.8 %copy-start.1 = (bf16[16,1024]{1,0:T(8,128)(2,1)S(1)}, bf16[16,1024]{1,0:T(8,128)(2,1)}, u32[]{:S(2)}) copy-start(bf16[16,1024]{1,0:T(8,128)(2,1)} %param.23) | copy-start | bytes 98308
  9.6 10.8 %copy-start.5 = (f32[1024]{0:T(1024)S(1)}, f32[1024]{0:T(1024)}, u32[]{:S(2)}) copy-start(f32[1024]{0:T(1024)} %param.28) | copy-start | bytes 12292
  19.2 3.7 %copy-start.3 = (f32[16,1,1024]{2,1,0:T(1,128)S(1)}, f32[16,1,1024]{2,1,0:T(1,128)}, u32[]{:S(2)}) copy-start(f32[16,1,1024]{2,1,0:T(1,128)} %shard_map.238) | copy-start | bytes 196612
  22.4 37.4 %copy-start.4 = (bf16[16,1024]{1,0:T(8,128)(2,1)}, bf16[16,1024]{1,0:T(8,128)(2,1)S(1)}, u32[]{:S(2)}) copy-start(bf16[16,1024]{1,0:T(8,128)(2,1)S(1)} %convolution_convert_fusion) | copy-start | bytes 98308
  22.4 1.2 %copy-start.7 = (f32[1024]{0:T(1024)S(1)}, f32[1024]{0:T(1024)}, u32[]{:S(2)}) copy-start(f32[1024]{0:T(1024)} %param.33) | copy-start | bytes 12292
  22.4 1.3 %copy-start.6 = (f32[16,6]{0,1:T(8,128)S(1)}, f32[16,6]{0,1:T(8,128)}, u32[]{:S(2)}) copy-start(f32[16,6]{0,1:T(8,128)} %param.35) | copy-start | bytes 1156
  22.4 1.3 %copy-start.8 = (s32[16,6]{0,1:T(8,128)S(1)}, s32[16,6]{0,1:T(8,128)}, u32[]{:S(2)}) copy-start(s32[16,6]{0,1:T(8,128)} %param.34) | copy-start | bytes 1156
  23.6 1.0 %copy-start.2 = (f32[16,1024]{1,0:T(8,128)}, f32[16,1024]{1,0:T(8,128)S(1)}, u32[]{:S(2)}) copy-start(f32[16,1024]{1,0:T(8,128)S(1)} %get-tuple-element.4.residual_ref) | copy-start | bytes 196612
